TPU v7x, 32 devices: a whole 2x2x4 slice. The times are simulated.
32 devices in a mesh: sp: 8 (over z, x), tp: 4 (over y, core).
Axes of the slice: x: 2, y: 2, z: 4, core: 2. Of those that a mesh axis runs over, the one named last changes fastest.
Arguments:
- resid: bfloat16 [3072, 2048], P('sp'), may hold values from -6 to 6
- cotangent: bfloat16 [3072, 2048], P('sp'), may hold values from -0.59765625 to 0.59765625
- routes: int32 [3072, 2], P('sp'), may hold values from 0 to 7, all different within a row; in each aligned block of 384 rows (0 to 383, 384 to 767, ...) at most 192 rows name the same one
- route_weight: float32 [3072, 2], P('sp'), may hold values from 0.3 to 2.2
- w_gate: bfloat16 [8, 2048, 1024], P('sp', None, 'tp'), may hold values from -0.125 to 0.125
- w_up: bfloat16 [8, 2048, 1024], P('sp', None, 'tp'), may hold values from -0.125 to 0.125
- w_down: bfloat16 [8, 1024, 2048], P('sp', 'tp'), may hold values from -0.1875 to 0.1875
- out_proj: bfloat16 [2048, 2816], P(None, 'tp'), may hold values from -0.109375 to 0.109375
- gate_pre: bfloat16 [3072, 2816], P('sp', 'tp'), may hold values from -8 to 8
- log_decay: float32 [3072, 2816], P('sp', 'tp'), may hold values from -1 to 0
- state_before: float32 [3072, 2816], P('sp', 'tp'), may hold values from -6 to 6
- step_input: bfloat16 [3072, 2816], P('sp', 'tp'), may hold values from -6 to 6
Outputs:
- grad_gate: float32 [8, 2048, 1024], P('sp', None, 'tp')
- grad_up: float32 [8, 2048, 1024], P('sp', None, 'tp')
- grad_down: float32 [8, 1024, 2048], P('sp', 'tp')
- grad_proj: float32 [2048, 2816], P('sp', 'tp')
- grad_gate_pre: bfloat16 [3072, 2816], P('sp', 'tp')
- grad_step_input: float32 [3072, 2816], P('sp', 'tp')
- grad_log_decay: float32 [3072, 2816], P('sp', 'tp')
Inputs may be any that keep to these rules, and one draw needn't show every extreme that they name: `routes`: each row names 2 different experts. In the rows of one device no expert is named more than 192 times; some expert is named exactly 192 times in the rows of some devices.
All inputs are finite; a program needn't handle non-finite values.
Results may differ from a plain program's by a relative error of at most 0.02.
Values may be sent and summed in bfloat16 or wider, within the bound.
A program may use at most 128 MiB of HBM per device.

v0:
```python
import jax
import jax.numpy as jnp
from jax import lax
from jax.sharding import PartitionSpec as P


def carried_in(part, axis, combine, identity):
    count = lax.axis_size(axis)
    place = lax.axis_index(axis)
    ahead = count - 1 - place
    gathered = jax.tree.map(lambda a: lax.all_gather(a, axis), part)
    state = jax.tree.map(lambda a, e: jnp.zeros_like(a) + jnp.asarray(e, a.dtype), part, identity)

    def one(turn, state):
        source = count - 1 - turn
        return combine(
            state, jax.tree.map(lambda a: lax.dynamic_index_in_dim(a, source, 0, False), gathered)
        )

    return lax.fori_loop(0, ahead, one, state)


def expert_work(in_rows, cot_rows, gate_w, up_w, down_w):
    gate_act = jnp.dot(in_rows, gate_w, preferred_element_type=jnp.float32)
    up_act = jnp.dot(in_rows, up_w, preferred_element_type=jnp.float32)
    sigmoid_a = jax.nn.sigmoid(gate_act)
    hidden = (jax.nn.silu(gate_act) * up_act).astype(jnp.bfloat16)
    grad_down = lax.dot_general(
        hidden, cot_rows, (((0,), (0,)), ((), ())), preferred_element_type=jnp.float32
    )
    d_hidden = lax.dot_general(
        cot_rows, down_w, (((1,), (1,)), ((), ())), preferred_element_type=jnp.float32
    )
    slope = sigmoid_a * (1.0 + gate_act * (1.0 - sigmoid_a))
    d_gate_act = (d_hidden * up_act * slope).astype(jnp.bfloat16)
    d_up_act = (d_hidden * jax.nn.silu(gate_act)).astype(jnp.bfloat16)
    grad_gate = lax.dot_general(
        in_rows, d_gate_act, (((0,), (0,)), ((), ())), preferred_element_type=jnp.float32
    )
    grad_up = lax.dot_general(
        in_rows, d_up_act, (((0,), (0,)), ((), ())), preferred_element_type=jnp.float32
    )
    partial_value = lax.dot_general(
        d_gate_act, gate_w, (((1,), (1,)), ((), ())), preferred_element_type=jnp.float32
    )
    partial_value = partial_value + lax.dot_general(
        d_up_act, up_w, (((1,), (1,)), ((), ())), preferred_element_type=jnp.float32
    )
    rounded = lax.optimization_barrier(partial_value.astype(jnp.bfloat16))
    return (grad_gate[None], grad_up[None], grad_down[None], rounded.astype(jnp.float32))


def gather_slots(resid_part, cot_part, slot_token, slot_weight, groups, capacity):
    col_width = resid_part.shape[1]
    resid_pad = jnp.concatenate([resid_part, jnp.zeros((1, col_width), jnp.bfloat16)], axis=0)
    cot_pad = jnp.concatenate([cot_part, jnp.zeros((1, col_width), jnp.bfloat16)], axis=0)
    send_rows = resid_pad[slot_token].reshape(groups, capacity, col_width)
    send_cot = (slot_weight[:, None] * cot_pad[slot_token].astype(jnp.float32)).astype(jnp.bfloat16)
    return (send_rows, send_cot.reshape(groups, capacity, col_width))


def combine_slots(returned, cot_part, slot_ids, tok_rows, top_count):
    col_width = returned.shape[2]
    flat_back = returned.reshape(-1, col_width)
    routed = jnp.sum(
        flat_back[slot_ids].astype(jnp.float32).reshape(tok_rows, top_count, col_width), axis=1
    )
    return (cot_part.astype(jnp.float32) + routed).astype(jnp.bfloat16)


def reverse_link(former, latter):
    return (former[0] * latter[0], latter[0] * former[1] + latter[1])


def compose(earlier, later):
    return (later[0] * earlier[0], later[0] * earlier[1] + later[1])


def on_device(
    resid,
    cotangent,
    routes,
    route_weight,
    w_gate,
    w_up,
    w_down,
    out_proj,
    gate_pre,
    log_decay,
    state_before,
    step_input,
):
    tok_rows, model_width = resid.shape
    top_count = routes.shape[1]
    groups = lax.axis_size("sp")
    capacity = 2 * tok_rows * top_count // groups
    flat_ids = routes.reshape(-1)
    onehot = (flat_ids[:, None] == jnp.arange(groups, dtype=jnp.int32)[None, :]).astype(jnp.int32)
    ranking = jnp.sum((jnp.cumsum(onehot, axis=0) - onehot) * onehot, axis=1)
    slot_ids = flat_ids * capacity + ranking
    member = slot_ids[None, :] == jnp.arange(groups * capacity, dtype=jnp.int32)[:, None]
    token_ids = jnp.arange(tok_rows * top_count, dtype=jnp.int32) // top_count
    filled = jnp.any(member, axis=1)
    slot_token = jnp.where(
        filled, jnp.sum(jnp.where(member, token_ids[None, :], 0), axis=1), tok_rows
    )
    slot_weight = jnp.sum(jnp.where(member, route_weight.reshape(-1)[None, :], 0.0), axis=1)
    col_width = model_width // lax.axis_size("tp")
    col_start = lax.axis_index("tp") * col_width
    cot_part = lax.dynamic_slice_in_dim(cotangent, col_start, col_width, 1)
    resid_part = lax.dynamic_slice_in_dim(resid, col_start, col_width, 1)
    send_rows, send_cot = gather_slots(
        resid_part, cot_part, slot_token, slot_weight, groups, capacity
    )
    got_rows, got_cot = (
        lax.all_to_all(send_rows, "sp", split_axis=0, concat_axis=0, tiled=True),
        lax.all_to_all(send_cot, "sp", split_axis=0, concat_axis=0, tiled=True),
    )
    full_rows, full_cot = (
        lax.all_gather(got_rows, "tp", axis=2, tiled=True),
        lax.all_gather(got_cot, "tp", axis=2, tiled=True),
    )
    grad_gate, grad_up, grad_down, partial_value = expert_work(
        full_rows.reshape(-1, model_width),
        full_cot.reshape(-1, model_width),
        w_gate[0],
        w_up[0],
        w_down[0],
    )
    summed = lax.psum_scatter(
        partial_value.reshape(groups, capacity, model_width).astype(jnp.bfloat16),
        "tp",
        scatter_dimension=2,
        tiled=True,
    )
    returned = lax.all_to_all(summed, "sp", split_axis=0, concat_axis=0, tiled=True)
    part_grad = combine_slots(returned, cot_part, slot_ids, tok_rows, top_count)
    resid_grad = lax.all_gather(part_grad, "tp", axis=1, tiled=True)
    decays = jnp.exp(log_decay)
    states = decays * state_before + step_input.astype(jnp.float32)
    gelu_val, gelu_back = jax.vjp(jax.nn.gelu, gate_pre.astype(jnp.float32))
    mixed = (gelu_val * states).astype(jnp.bfloat16)
    d_mixed = jnp.dot(resid_grad, out_proj, preferred_element_type=jnp.float32)
    grad_gate_pre = gelu_back(d_mixed * states)[0].astype(jnp.bfloat16)
    grad_proj = lax.psum_scatter(
        lax.dot_general(
            resid_grad, mixed, (((0,), (0,)), ((), ())), preferred_element_type=jnp.float32
        ).astype(jnp.bfloat16),
        "sp",
        scatter_dimension=0,
        tiled=True,
    ).astype(jnp.float32)
    direct = d_mixed * gelu_val
    channels = direct.shape[1]
    following = jnp.concatenate([decays[1:], jnp.ones((1, channels), jnp.float32)], axis=0)
    products, local_vals = lax.associative_scan(
        reverse_link, (jnp.flip(following, 0), jnp.flip(direct, 0)), axis=0
    )
    products = jnp.flip(products, 0)
    local_vals = jnp.flip(local_vals, 0)
    out_scale = decays[0] * products[0]
    out_shift = decays[0] * local_vals[0]
    identity = (jnp.ones((channels,), jnp.float32), jnp.zeros((channels,), jnp.float32))
    arriving = carried_in((out_scale, out_shift), "sp", compose, identity)
    grad_step_input = local_vals + products * arriving[1][None, :]
    grad_log_decay = grad_step_input * decays * state_before
    return (
        grad_gate,
        grad_up,
        grad_down,
        grad_proj,
        grad_gate_pre,
        grad_step_input,
        grad_log_decay,
    )


def solution(mesh):
    return jax.shard_map(
        on_device,
        mesh=mesh,
        in_specs=(
            P("sp", None),
            P("sp", None),
            P("sp", None),
            P("sp", None),
            P("sp", None, "tp"),
            P("sp", None, "tp"),
            P("sp", "tp", None),
            P(None, "tp"),
            P("sp", "tp"),
            P("sp", "tp"),
            P("sp", "tp"),
            P("sp", "tp"),
        ),
        out_specs=(
            P("sp", None, "tp"),
            P("sp", None, "tp"),
            P("sp", "tp", None),
            P("sp", "tp"),
            P("sp", "tp"),
            P("sp", "tp"),
            P("sp", "tp"),
        ),
        check_vma=False,
    )
```

profile of v0, /device:TPU:0, one launch (start us, length us, event | category | flops | bytes accessed | tf_op | source)
XLA Modules:
  0.0 636.6 jit_solution(3551452803279779135)
XLA Ops:
  14.0 5.4 gather_fusion
  19.4 44.4 %all_to_all.15 = bf16[8,192,512]{2,1,0:T(8,128)(2,1)} all-to-all(bf16[8,192,512]{2,1,0:T(8,128)(2,1)} %bitcast.63), channel_id=1, replica_groups=mesh['sp'=8,'tp'=4] {'sp'}, dimensions={0} | all-to-all | bytes 3145728 | tf_op jit(solution)/shard_map/all_to_all | solution.py:116
  64.9 5.4 gather_fusion.1
  73.2 40.2 %all_to_all.16 = bf16[8,192,512]{2,1,0:T(8,128)(2,1)} all-to-all(bf16[8,192,512]{2,1,0:T(8,128)(2,1)S(1)} %fusion.1), channel_id=1, replica_groups=mesh['sp'=8,'tp'=4] {'sp'}, dimensions={0} | all-to-all | bytes 3145728 | tf_op jit(solution)/shard_map/all_to_all | solution.py:117
  113.7 6.1 fusion.14
  122.8 36.1 %all-gather.8.cloned.1.call-done = bf16[8,192,2048]{2,1,0:T(8,128)(2,1)} async-done(((bf16[8,192,512]{2,1,0:T(8,128)(2,1)}), bf16[8,192,2048]{2,1,0:T(8,128)(2,1)}) %all-gather.8.cloned.1.call-update) | async-done | bytes 6291472 | tf_op jit(solution)/shard_map/all_gather | solution.py:121
  158.9 6.4 %multiply_convert_fusion.1 = (bf16[1536,256]{1,0:T(8,128)(2,1)S(1)}, bf16[1536,256]{1,0:T(8,128)(2,1)S(1)}) fusion(f32[1536,256]{1,0:T(8,128)} %fusion.14, f32[1536,256]{1,0:T(8,128)} %fusion.17, bf16[1536,2048]{1,0:T(8,128)(2,1)} %bitcast.72, bf16[1,256,2048]{2,1,0:T(8,128)(2,1)} %param.20), kind=kOutput, calls=%fused_computation.24 | convolution fusion | flops 1615724544 | bytes 12058624 | tf_op jit(solution)/shard_map/dot_general | solution.py:31
  171.7 58.0 %reduce-scatter.3.cloned.1.call-done = bf16[8,192,512]{2,1,0:T(8,128)(2,1)} async-done(((bf16[8,192,2048]{2,1,0:T(8,128)(2,1)}), bf16[8,192,512]{2,1,0:T(8,128)(2,1)}) %reduce-scatter.3.cloned.1.call-update) | async-done | bytes 1572880 | tf_op jit(solution)/shard_map/reduce_scatter | solution.py:130
  229.7 5.5 all-to-all-start.2
  235.8 36.3 %all-to-all-done.2 = bf16[8,192,512]{2,1,0:T(8,128)(2,1)} async-done(((bf16[8,192,512]{2,1,0:T(8,128)(2,1)}), bf16[8,192,512]{2,1,0:T(8,128)(2,1)}, u32[]{:S(2)}, u32[]{:S(2)}) %all-to-all-start.2) | async-done | bytes 1572896 | tf_op jit(solution)/shard_map/all_to_all | solution.py:136
  272.1 5.0 gather_fusion.2
  310.0 6.8 %slice.280 = f32[191,704]{1,0:T(8,128)} reverse(f32[191,704]{1,0:T(8,128)} %slice.279), dimensions={0} | reverse | bytes 1075712 | tf_op jit(solution)/shard_map/slice | solution.py:156
  316.8 6.7 %slice.289 = f32[192,704]{1,0:T(8,128)} reverse(f32[192,704]{1,0:T(8,128)} %slice.288), dimensions={0} | reverse | bytes 1081344 | tf_op jit(solution)/shard_map/slice | solution.py:156
  323.5 6.6 %slice.282 = f32[192,704]{1,0:T(8,128)} reverse(f32[192,704]{1,0:T(8,128)} %slice.281), dimensions={0} | reverse | bytes 1081344 | tf_op jit(solution)/shard_map/slice | solution.py:156
  330.1 6.3 convolution_bitcast_fusion.2
  336.5 6.2 convolution_bitcast_fusion.1
  356.9 6.6 %slice.286 = f32[192,704]{1,0:T(8,128)} reverse(f32[192,704]{1,0:T(8,128)} %slice.285), dimensions={0} | reverse | bytes 1081344 | tf_op jit(solution)/shard_map/slice | solution.py:156
  414.4 6.0 convolution_convert_fusion
  492.6 6.8 %slice.344 = f32[191,704]{1,0:T(8,128)} reverse(f32[191,704]{1,0:T(8,128)} %slice.343), dimensions={0} | reverse | bytes 1075712 | tf_op jit(solution)/shard_map/slice | solution.py:156
  522.1 9.9 %rev.9 = f32[384,704]{1,0:T(8,128)} reverse(f32[384,704]{1,0:T(8,128)} %add.308), dimensions={0} | reverse | bytes 2162688 | tf_op jit(solution)/shard_map/jit(_flip)/rev | solution.py:160
  543.3 9.8 %rev.10 = f32[384,704]{1,0:T(8,128)} reverse(f32[384,704]{1,0:T(8,128)} %add.316), dimensions={0} | reverse | bytes 2162688 | tf_op jit(solution)/shard_map/jit(_flip)/rev | solution.py:159
  554.0 30.5 %all-gather = f32[8,1,704]{2,1,0:T(1,128)S(1)} all-gather(f32[1,1,704]{2,1,0:T(1,128)S(1)} %get-tuple-element.121), channel_id=1, replica_groups=mesh['sp'=8,'tp'=4] {'sp'}, dimensions={0}, use_global_device_ids=true | all-gather | bytes 25344 | tf_op jit(solution)/shard_map/all_gather | solution.py:11
  584.5 30.5 %all-gather.1 = f32[8,1,704]{2,1,0:T(1,128)S(1)} all-gather(f32[1,1,704]{2,1,0:T(1,128)S(1)} %get-tuple-element.120), channel_id=1, replica_groups=mesh['sp'=8,'tp'=4] {'sp'}, dimensions={0}, use_global_device_ids=true | all-gather | bytes 25344 | tf_op jit(solution)/shard_map/all_gather | solution.py:11
  615.5 5.0 multiply_multiply_fusion
  (294 shorter events, 235.4 us)
Async XLA Ops:
  7.2 338.7 %copy-start = (bf16[2048,704]{0,1:T(8,128)(2,1)S(1)}, bf16[2048,704]{0,1:T(8,128)(2,1)}, u32[]{:S(2)}) copy-start(bf16[2048,704]{0,1:T(8,128)(2,1)} %param.21) | copy-start | bytes 8650756
  7.2 106.5 %all-gather.6.cloned.1.call-start = ((), (), s32[]{:S(2)}) async-start(), calls=%async_computation.5 | async-start | bytes 7864320 | tf_op jit(solution)/shard_map/all_gather | solution.py:120
  63.8 95.1 %all-gather.8.cloned.1.call-start = ((), (), s32[]{:S(2)}) async-start(), calls=%async_computation.6 | async-start | bytes 7864320 | tf_op jit(solution)/shard_map/all_gather | solution.py:121
  113.4 116.3 %reduce-scatter.3.cloned.1.call-start = ((), (), s32[]{:S(2)}) async-start(), calls=%async_computation.7 | async-start | bytes 7864320 | tf_op jit(solution)/shard_map/reduce_scatter | solution.py:130
  158.9 6.4 %copy-start.16 = (bf16[1,2048,256]{2,1,0:T(8,128)(2,1)S(1)}, bf16[1,2048,256]{2,1,0:T(8,128)(2,1)}, u32[]{:S(2)}) copy-start(bf16[1,2048,256]{2,1,0:T(8,128)(2,1)} %param.18) | copy-start | bytes 3145732
  171.7 63.8 %copy-start.31 = (s32[384,2]{0,1:T(2,128)S(1)}, s32[384,2]{0,1:T(2,128)}, u32[]{:S(2)}) copy-start(s32[384,2]{0,1:T(2,128)} %param.16) | copy-start | bytes 9220
  229.7 42.4 %all-to-all-start.2 = ((bf16[8,192,512]{2,1,0:T(8,128)(2,1)}), bf16[8,192,512]{2,1,0:T(8,128)(2,1)}, u32[]{:S(2)}, u32[]{:S(2)}) async-start(bf16[8,192,512]{2,1,0:T(8,128)(2,1)} %reduce-scatter.3.cloned.1.call-done), calls=%async_computation.3 | async-start | bytes 3145728 | tf_op jit(solution)/shard_map/all_to_all | solution.py:136
  235.2 110.7 %all-gather.10.cloned.1.call-start = ((), (), s32[]{:S(2)}) async-start(), calls=%async_computation.8 | async-start | bytes 1966080 | tf_op jit(solution)/shard_map/all_gather | solution.py:138
  286.3 341.5 %reduce-scatter.5.cloned.1.call-start = ((), (), s32[]{:S(2)}) async-start(), calls=%async_computation.9 | async-start | bytes 3244032 | tf_op jit(solution)/shard_map/reduce_scatter | solution.py:145
  305.1 40.8 %copy-start.8 = (bf16[384,704]{1,0:T(8,128)(2,1)}, bf16[384,704]{1,0:T(8,128)(2,1)S(1)}, u32[]{:S(2)}) copy-start(bf16[384,704]{1,0:T(8,128)(2,1)S(1)} %copy.98) | copy-start | bytes 1622020
  330.1 6.3 copy-start.20
  330.1 12.5 %slice-start = ((s8[6291456]{0:T(1024)(128)(4,1)}), s8[4194304]{0:T(1024)(128)(4,1)S(1)}, s32[]{:S(2)}) async-start(s8[6291456]{0:T(1024)(128)(4,1)} %bitcast.73), calls=%async_computation.10 | async-start | bytes 8388608
  336.4 6.2 copy-start.36
  336.4 6.2 copy-start.37
  442.8 20.7 %copy-start.24 = (f32[5,704]{1,0:T(8,128)S(1)}, f32[5,704]{1,0:T(8,128)}, u32[]{:S(2)}) copy-start(f32[5,704]{1,0:T(8,128)} %slice.314) | copy-start | bytes 42244
  449.7 16.6 %copy-start.23 = (f32[11,704]{1,0:T(8,128)S(1)}, f32[11,704]{1,0:T(8,128)}, u32[]{:S(2)}) copy-start(f32[11,704]{1,0:T(8,128)} %slice.308) | copy-start | bytes 92932
  458.4 8.8 %copy-start.30 = (f32[1,704]{1,0:T(1,128)S(1)}, f32[1,704]{1,0:T(1,128)}, u32[]{:S(2)}) copy-start(f32[1,704]{1,0:T(1,128)} %slice.399) | copy-start | bytes 8452
  458.4 9.7 %copy-start.29 = (f32[1,704]{1,0:T(1,128)S(1)}, f32[1,704]{1,0:T(1,128)}, u32[]{:S(2)}) copy-start(f32[1,704]{1,0:T(1,128)} %slice.374) | copy-start | bytes 8452
  460.4 8.4 %copy-start.21 = (f32[23,704]{1,0:T(8,128)S(1)}, f32[23,704]{1,0:T(8,128)}, u32[]{:S(2)}) copy-start(f32[23,704]{1,0:T(8,128)} %slice.302) | copy-start | bytes 194308
  460.4 8.4 %copy-start.22 = (f32[23,704]{1,0:T(8,128)S(1)}, f32[23,704]{1,0:T(8,128)}, u32[]{:S(2)}) copy-start(f32[23,704]{1,0:T(8,128)} %slice.337) | copy-start | bytes 194308
  468.8 6.3 copy-start.28
  490.0 12.1 %copy-start.25 = (f32[1,704]{1,0:T(1,128)S(1)}, f32[1,704]{1,0:T(1,128)}, u32[]{:S(2)}) copy-start(f32[1,704]{1,0:T(1,128)} %slice.371) | copy-start | bytes 8452
  522.1 9.9 %copy-start.11 = (f32[191,704]{1,0:T(8,128)S(1)}, f32[191,704]{1,0:T(8,128)}, u32[]{:S(2)}) copy-start(f32[191,704]{1,0:T(8,128)} %get-tuple-element.122) | copy-start | bytes 1613572
  543.3 72.2 %copy-start.9 = (bf16[384,704]{1,0:T(8,128)(2,1)S(1)}, bf16[384,704]{1,0:T(8,128)(2,1)}, u32[]{:S(2)}) copy-start(bf16[384,704]{1,0:T(8,128)(2,1)} %copy-done.8) | copy-start | bytes 1622020
  (22 other events, 78.0 us)
Sparse Core Ops, SparseCore 0:
  63.9 45.3 all-gather.5
  113.5 45.3 all-gather.7
  171.8 57.8 reduce-scatter.2
  286.4 17.7 all-gather.9
  420.5 71.2 reduce-scatter.4
where the time goes:
time: 649 us; the launch traced here: 637 us
  local copies, waits for them, and re-layouts  228 us (35%)
  blocking collectives  146 us (22%)
  waiting for transfers between devices  131 us (20%)
  other arithmetic  63.8 us (10%)
  matrix products  47.8 us (7%)
  between operations  15 us (2%)
    slice x61, local copies, waits for them, and re-layouts, on_device(): lax.associative_scan(reverse_link, (jnp.flip(following, 0), jnp.flip(dire...  129 us
    all_gather x2, blocking collectives, carried_in(): gathered = jax.tree.map(lambda a: lax.all_gather(a, axis), part)  61 us
    reduce_scatter x1, waiting for transfers between devices, on_device(): lax.psum_scatter(partial_value.reshape(groups, capacity, model_width).ast...  58 us
    all_to_all x1, blocking collectives, on_device(): lax.all_to_all(send_rows, 'sp', split_axis=0, concat_axis=0, tiled=True)  44.4 us
    all_to_all x1, blocking collectives, on_device(): lax.all_to_all(send_cot, 'sp', split_axis=0, concat_axis=0, tiled=True)  40.2 us
    all_to_all x1, waiting for transfers between devices, on_device(): lax.all_to_all(summed, 'sp', split_axis=0, concat_axis=0, tiled=True)  36.3 us
    all_gather x1, waiting for transfers between devices, on_device(): lax.all_gather(got_cot, 'tp', axis=2, tiled=True)  36.1 us
    pad x30, local copies, waits for them, and re-layouts, on_device(): lax.associative_scan(reverse_link, (jnp.flip(following, 0), jnp.flip(dire...  33.1 us
  transfers between devices with their start and end apart: 6, of which 3 were waited for; matrix products, arithmetic and copies ran while one was open for 35% of the time, Pallas kernels for 0%

commit v1 on v0

--- a/solution.py
+++ b/solution.py
@@ -1,23 +1,154 @@
+import functools
+
 import jax
 import jax.numpy as jnp
 from jax import lax
 from jax.sharding import PartitionSpec as P
 
 
-def carried_in(part, axis, combine, identity):
-    count = lax.axis_size(axis)
-    place = lax.axis_index(axis)
-    ahead = count - 1 - place
-    gathered = jax.tree.map(lambda a: lax.all_gather(a, axis), part)
-    state = jax.tree.map(lambda a, e: jnp.zeros_like(a) + jnp.asarray(e, a.dtype), part, identity)
-
-    def one(turn, state):
-        source = count - 1 - turn
-        return combine(
-            state, jax.tree.map(lambda a: lax.dynamic_index_in_dim(a, source, 0, False), gathered)
+from jax.experimental import pallas as pl
+from jax.experimental.pallas import tpu as pltpu
+
+MESH_IDS = pl.DeviceIdType.MESH
+SUBLANES = 8
+CUBIC = 0.044715
+TANH_SCALE = 0.7978845608028654
+
+
+def recurrence_kernel(
+    dm_ref, pre_ref, ld_ref, sb_ref, si_ref, ggp_ref, loc_ref, prod_ref, edge_ref, carry
+):
+    rows, channels = dm_ref.shape
+
+    @pl.when(pl.program_id(0) == 0)
+    def _():
+        carry[0:1, :] = jnp.zeros((1, channels), jnp.float32)
+        carry[1:2, :] = jnp.ones((1, channels), jnp.float32)
+
+    row = lax.broadcasted_iota(jnp.int32, (SUBLANES, channels), 0)
+
+    def ahead(x, k, fill):
+        return jnp.where(row < SUBLANES - k, pltpu.roll(x, SUBLANES - k, 0), fill)
+
+    def pair(j, state):
+        shift_in, scale_in = state
+        start = pl.multiple_of(rows - 2 * SUBLANES * (j + 1), 2 * SUBLANES)
+        both = pl.ds(start, 2 * SUBLANES)
+        pre = pre_ref[both, :].astype(jnp.float32)
+        step_in = si_ref[both, :].astype(jnp.float32)
+        dm = dm_ref[both, :]
+        decay = jnp.exp(ld_ref[both, :])
+        state_val = decay * sb_ref[both, :] + step_in
+        square = pre * pre
+        tanh = jnp.tanh(TANH_SCALE * (pre + CUBIC * square * pre))
+        half = 0.5 * (1.0 + tanh)
+        slope = half + 0.5 * pre * (1.0 - tanh * tanh) * (
+            TANH_SCALE * (1.0 + 3.0 * CUBIC * square)
         )
-
-    return lax.fori_loop(0, ahead, one, state)
+        direct = dm * (pre * half)
+        ggp_ref[both, :] = (dm * state_val * slope).astype(jnp.bfloat16)
+        for part in (1, 0):
+            lo = part * SUBLANES
+            own = direct[lo : lo + SUBLANES]
+            scale = decay[lo : lo + SUBLANES]
+            shift = scale * own
+            for k in (1, 2, 4):
+                shift = shift + scale * ahead(shift, k, 0.0)
+                scale = scale * ahead(scale, k, 1.0)
+            shift = shift + scale * shift_in
+            scale = scale * scale_in
+            loc_ref[pl.ds(start + lo, SUBLANES), :] = own + ahead(shift, 1, shift_in)
+            prod_ref[pl.ds(start + lo, SUBLANES), :] = ahead(scale, 1, scale_in)
+            shift_in = shift[0:1]
+            scale_in = scale[0:1]
+        return (shift_in, scale_in)
+
+    shift_in, scale_in = lax.fori_loop(
+        0, rows // (2 * SUBLANES), pair, (carry[0:1, :], carry[1:2, :])
+    )
+    carry[0:1, :] = shift_in
+    carry[1:2, :] = scale_in
+    edge_ref[...] = jnp.where(row == 0, scale_in, shift_in)
+
+
+def local_recurrence(d_mixed, gate_pre, log_decay, state_before, step_input):
+    tokens, channels = d_mixed.shape
+    steps = 1
+    while tokens % (2 * steps * 2 * SUBLANES) == 0 and steps < 4:
+        steps = 2 * steps
+    block = pl.BlockSpec((tokens // steps, channels), lambda i: (steps - 1 - i, 0))
+    wide = jax.ShapeDtypeStruct((tokens, channels), jnp.float32)
+    return pl.pallas_call(
+        recurrence_kernel,
+        grid=(steps,),
+        in_specs=[block] * 5,
+        out_specs=[block] * 3 + [pl.BlockSpec((SUBLANES, channels), lambda i: (0, 0))],
+        out_shape=[
+            jax.ShapeDtypeStruct((tokens, channels), jnp.bfloat16),
+            wide,
+            wide,
+            jax.ShapeDtypeStruct((SUBLANES, channels), jnp.float32),
+        ],
+        scratch_shapes=[pltpu.VMEM((SUBLANES, channels), jnp.float32)],
+        compiler_params=pltpu.CompilerParams(dimension_semantics=("arbitrary",)),
+        cost_estimate=pl.CostEstimate(
+            flops=60 * tokens * channels,
+            bytes_accessed=28 * tokens * channels,
+            transcendentals=2 * tokens * channels,
+        ),
+        name="local_recurrence",
+    )(d_mixed, gate_pre, log_decay, state_before, step_input)
+
+
+def carry_kernel(count, edge_ref, out_ref, held, send_sem, recv_sem):
+    place = lax.axis_index("sp")
+    barrier = pltpu.get_barrier_semaphore()
+    for k in range(1, count):
+        pl.semaphore_signal(
+            barrier, inc=1, device_id={"sp": lax.rem(place + k, count)}, device_id_type=MESH_IDS
+        )
+    pl.semaphore_wait(barrier, count - 1)
+    sends = []
+    for k in range(1, count):
+        copy = pltpu.make_async_remote_copy(
+            src_ref=edge_ref,
+            dst_ref=held.at[k],
+            send_sem=send_sem.at[k],
+            recv_sem=recv_sem.at[k],
+            device_id={"sp": lax.rem(place + count - k, count)},
+            device_id_type=MESH_IDS,
+        )
+        copy.start()
+        sends.append(copy)
+    for copy in sends:
+        copy.wait()
+    value = jnp.zeros((1, edge_ref.shape[1]), jnp.float32)
+    for k in range(count - 1, 0, -1):
+        turn = held[k, 0:1, :] * value + held[k, 1:2, :]
+        value = jnp.where(place + k < count, turn, value)
+    out_ref[...] = jnp.broadcast_to(value, out_ref.shape)
+
+
+def carried_in(edge):
+    count = lax.axis_size("sp")
+    channels = edge.shape[1]
+    arriving = pl.pallas_call(
+        functools.partial(carry_kernel, count),
+        out_shape=jax.ShapeDtypeStruct((SUBLANES, channels), jnp.float32),
+        in_specs=[pl.BlockSpec(memory_space=pltpu.VMEM)],
+        out_specs=pl.BlockSpec(memory_space=pltpu.VMEM),
+        scratch_shapes=[
+            pltpu.VMEM((count, SUBLANES, channels), jnp.float32),
+            pltpu.SemaphoreType.DMA((count,)),
+            pltpu.SemaphoreType.DMA((count,)),
+        ],
+        compiler_params=pltpu.CompilerParams(collective_id=1, has_side_effects=True),
+        cost_estimate=pl.CostEstimate(
+            flops=20000, bytes_accessed=8000000, transcendentals=0
+        ),
+        name="carry_exchange",
+    )(edge)
+    return arriving[0:1]
 
 
 def expert_work(in_rows, cot_rows, gate_w, up_w, down_w):
@@ -66,14 +197,6 @@
         flat_back[slot_ids].astype(jnp.float32).reshape(tok_rows, top_count, col_width), axis=1
     )
     return (cot_part.astype(jnp.float32) + routed).astype(jnp.bfloat16)
-
-
-def reverse_link(former, latter):
-    return (former[0] * latter[0], latter[0] * former[1] + latter[1])
-
-
-def compose(earlier, later):
-    return (later[0] * earlier[0], later[0] * earlier[1] + later[1])
 
 
 def on_device(
@@ -138,10 +261,8 @@
     resid_grad = lax.all_gather(part_grad, "tp", axis=1, tiled=True)
     decays = jnp.exp(log_decay)
     states = decays * state_before + step_input.astype(jnp.float32)
-    gelu_val, gelu_back = jax.vjp(jax.nn.gelu, gate_pre.astype(jnp.float32))
-    mixed = (gelu_val * states).astype(jnp.bfloat16)
+    mixed = (jax.nn.gelu(gate_pre.astype(jnp.float32)) * states).astype(jnp.bfloat16)
     d_mixed = jnp.dot(resid_grad, out_proj, preferred_element_type=jnp.float32)
-    grad_gate_pre = gelu_back(d_mixed * states)[0].astype(jnp.bfloat16)
     grad_proj = lax.psum_scatter(
         lax.dot_general(
             resid_grad, mixed, (((0,), (0,)), ((), ())), preferred_element_type=jnp.float32
@@ -150,19 +271,11 @@
         scatter_dimension=0,
         tiled=True,
     ).astype(jnp.float32)
-    direct = d_mixed * gelu_val
-    channels = direct.shape[1]
-    following = jnp.concatenate([decays[1:], jnp.ones((1, channels), jnp.float32)], axis=0)
-    products, local_vals = lax.associative_scan(
-        reverse_link, (jnp.flip(following, 0), jnp.flip(direct, 0)), axis=0
-    )
-    products = jnp.flip(products, 0)
-    local_vals = jnp.flip(local_vals, 0)
-    out_scale = decays[0] * products[0]
-    out_shift = decays[0] * local_vals[0]
-    identity = (jnp.ones((channels,), jnp.float32), jnp.zeros((channels,), jnp.float32))
-    arriving = carried_in((out_scale, out_shift), "sp", compose, identity)
-    grad_step_input = local_vals + products * arriving[1][None, :]
+    grad_gate_pre, local_vals, products, edge = local_recurrence(
+        d_mixed, gate_pre, log_decay, state_before, step_input
+    )
+    arriving = carried_in(edge)
+    grad_step_input = local_vals + products * arriving
     grad_log_decay = grad_step_input * decays * state_before
     return (
         grad_gate,

time: 649 us -> 396 us (0.61); the launches traced: 637 us -> 395 us
  local copies, waits for them, and re-layouts: 228 us -> 41 us
  blocking collectives: 146 us -> 84.6 us
  other arithmetic: 63.8 us -> 17.8 us
  waiting for transfers between devices: 131 us -> 164 us
  Pallas kernels: 0 us -> 21.2 us
    slice x64 -> x3, local copies, waits for them, and re-layouts: 129 us -> 0.96 us  [the longest x1 0.75 us: carried_in(): return arriving[0:1]]
    all_gather x2 -> x0, blocking collectives: 61 us -> none  [carried_in(): gathered = jax.tree.map(lambda a: lax.all_gather(a, axis), part)]
    pad x30 -> x0, local copies, waits for them, and re-layouts: 33.1 us -> none  [on_device(): lax.associative_scan(reverse_link, (jnp.flip(following, 0), jnp.flip(dire...]
    reduce_scatter x1, waiting for transfers between devices: 0.01 us -> 24.9 us  [on_device(): lax.psum_scatter(lax.dot_general(resid_grad, mixed, (((0,), (0,)), ((), (...]
    pallas_call x0 -> x2, Pallas kernels: none -> 21.2 us  [the longest x1 15.4 us: carried_in(): pl.pallas_call(functools.partial(carry_kernel, count), out_shape=jax.Shap...]
    rev x2 -> x0, local copies, waits for them, and re-layouts: 19.8 us -> none  [the longest x1 9.94 us: on_device(): local_vals = jnp.flip(local_vals, 0)]
    mul x15 -> x0, other arithmetic: 19.7 us -> none  [reverse_link(): return (former[0] * latter[0], latter[0] * former[1] + latter[1])]
    add x23 -> x0, other arithmetic: 14.1 us -> none  [the longest x16 14 us: on_device(): lax.associative_scan(reverse_link, (jnp.flip(following, 0), jnp.flip(dire...]
  transfers between devices with their start and end apart: 6 -> 6, of which waited for: 3 -> 5; matrix products, arithmetic and copies ran while one was open for 35% -> 15% of each run, Pallas kernels for 0% -> 5%
where the time goes in v1:
time: 396 us; the launch traced here: 395 us
  waiting for transfers between devices  164 us (41%)
  blocking collectives  84.6 us (21%)
  matrix products  46 us (12%)
  local copies, waits for them, and re-layouts  41 us (10%)
  Pallas kernels  21.2 us (5%)
  other arithmetic  17.8 us (4%)
  between operations  14.1 us (4%)
  starting transfers between devices  6.11 us (2%)
    reduce_scatter x1, waiting for transfers between devices, on_device(): lax.psum_scatter(partial_value.reshape(groups, capacity, model_width).ast...  58 us
    all_to_all x1, blocking collectives, on_device(): lax.all_to_all(send_rows, 'sp', split_axis=0, concat_axis=0, tiled=True)  44.4 us
    all_to_all x1, blocking collectives, on_device(): lax.all_to_all(send_cot, 'sp', split_axis=0, concat_axis=0, tiled=True)  40.2 us
    all_to_all x1, waiting for transfers between devices, on_device(): lax.all_to_all(summed, 'sp', split_axis=0, concat_axis=0, tiled=True)  36.3 us
    all_gather x1, waiting for transfers between devices, on_device(): lax.all_gather(got_cot, 'tp', axis=2, tiled=True)  36 us
    reduce_scatter x1, waiting for transfers between devices, on_device(): lax.psum_scatter(lax.dot_general(resid_grad, mixed, (((0,), (0,)), ((), (...  24.9 us
    unnamed x43, local copies, waits for them, and re-layouts  17.4 us
    pallas_call x1, Pallas kernels, carried_in(): pl.pallas_call(functools.partial(carry_kernel, count), out_shape=jax.Shap...  15.4 us
  transfers between devices with their start and end apart: 6, of which 5 were waited for; matrix products, arithmetic and copies ran while one was open for 15% of the time, Pallas kernels for 5%

profile of v1, /device:TPU:0, one launch (start us, length us, event | category | flops | bytes accessed | tf_op | source)
XLA Modules:
  0.0 395.3 jit_solution(5258477847060662153)
XLA Ops:
  14.0 5.4 %gather_fusion = bf16[1536,512]{1,0:T(8,128)(2,1)} fusion(bf16[385,512]{1,0:T(8,128)(2,1)S(1)} %concatenate.6, s32[2048]{0:T(1024)S(1)} %pad_clamp_fusion), kind=kCustom, calls=%fused_computation | custom fusion | bytes 3151872 | tf_op jit(solution)/shard_map/gather | solution.py:188
  19.4 44.4 %all_to_all.15 = bf16[8,192,512]{2,1,0:T(8,128)(2,1)} all-to-all(bf16[8,192,512]{2,1,0:T(8,128)(2,1)} %bitcast.53), channel_id=1, replica_groups=mesh['sp'=8,'tp'=4] {'sp'}, dimensions={0} | all-to-all | bytes 3145728 | tf_op jit(solution)/shard_map/all_to_all | solution.py:239
  64.9 5.4 %gather_fusion.1 = bf16[1536,512]{1,0:T(8,128)(2,1)} fusion(bf16[385,512]{1,0:T(8,128)(2,1)S(1)} %concatenate.7, s32[2048]{0:T(1024)S(1)} %pad_clamp_fusion), kind=kCustom, calls=%fused_computation.1 | custom fusion | bytes 3151872 | tf_op jit(solution)/shard_map/gather | solution.py:189
  73.2 40.2 %all_to_all.16 = bf16[8,192,512]{2,1,0:T(8,128)(2,1)} all-to-all(bf16[8,192,512]{2,1,0:T(8,128)(2,1)S(1)} %fusion.1), channel_id=1, replica_groups=mesh['sp'=8,'tp'=4] {'sp'}, dimensions={0} | all-to-all | bytes 3145728 | tf_op jit(solution)/shard_map/all_to_all | solution.py:240
  113.7 6.1 %fusion.12 = f32[1536,256]{1,0:T(8,128)} fusion(bf16[1536,2048]{1,0:T(8,128)(2,1)} %bitcast.56, bf16[1,2048,256]{2,1,0:T(8,128)(2,1)} %param.16), kind=kOutput, calls=%fused_computation.34 | convolution fusion | flops 1610612736 | bytes 8912896 | tf_op jit(solution)/shard_map/dot_general | solution.py:155
  119.8 3.0 fusion.15
  122.8 36.0 %all-gather.6.cloned.1.call-done = bf16[8,192,2048]{2,1,0:T(8,128)(2,1)} async-done(((bf16[8,192,512]{2,1,0:T(8,128)(2,1)}), bf16[8,192,2048]{2,1,0:T(8,128)(2,1)}) %all-gather.6.cloned.1.call-update) | async-done | bytes 6291472 | tf_op jit(solution)/shard_map/all_gather | solution.py:244
  158.9 6.4 %multiply_convert_fusion.1 = (bf16[1536,256]{1,0:T(8,128)(2,1)S(1)}, bf16[1536,256]{1,0:T(8,128)(2,1)S(1)}) fusion(f32[1536,256]{1,0:T(8,128)} %fusion.12, f32[1536,256]{1,0:T(8,128)} %fusion.15, bf16[1536,2048]{1,0:T(8,128)(2,1)} %bitcast.60, bf16[1,256,2048]{2,1,0:T(8,128)(2,1)} %param.18), kind=kOutput, calls=%fused_computation.19 | convolution fusion | flops 1615724544 | bytes 12058624 | tf_op jit(solution)/shard_map/dot_general | solution.py:162
  167.2 4.4 %add_convert_fusion = bf16[1536,2048]{1,0:T(8,128)(2,1)} fusion(f32[1536,2048]{1,0:T(8,128)S(1)} %fusion.10, bf16[1536,256]{1,0:T(8,128)(2,1)S(1)} %get-tuple-element.38, bf16[1,2048,256]{2,1,0:T(8,128)(2,1)S(1)} %copy-done.6), kind=kOutput, calls=%fused_computation.3 | convolution fusion | flops 1616904192 | bytes 20709376 | tf_op jit(solution)/shard_map/dot_general | solution.py:177
  171.7 58.0 %reduce-scatter.3.cloned.1.call-done = bf16[8,192,512]{2,1,0:T(8,128)(2,1)} async-done(((bf16[8,192,2048]{2,1,0:T(8,128)(2,1)}), bf16[8,192,512]{2,1,0:T(8,128)(2,1)}) %reduce-scatter.3.cloned.1.call-update) | async-done | bytes 1572880 | tf_op jit(solution)/shard_map/reduce_scatter | solution.py:253
  229.7 5.5 %all-to-all-start.2 = ((bf16[8,192,512]{2,1,0:T(8,128)(2,1)}), bf16[8,192,512]{2,1,0:T(8,128)(2,1)}, u32[]{:S(2)}, u32[]{:S(2)}) async-start(bf16[8,192,512]{2,1,0:T(8,128)(2,1)} %reduce-scatter.3.cloned.1.call-done), calls=%async_computation.3 | async-start | bytes 3145728 | tf_op jit(solution)/shard_map/all_to_all | solution.py:259
  235.8 36.3 %all-to-all-done.2 = bf16[8,192,512]{2,1,0:T(8,128)(2,1)} async-done(((bf16[8,192,512]{2,1,0:T(8,128)(2,1)}), bf16[8,192,512]{2,1,0:T(8,128)(2,1)}, u32[]{:S(2)}, u32[]{:S(2)}) %all-to-all-start.2) | async-done | bytes 1572896 | tf_op jit(solution)/shard_map/all_to_all | solution.py:259
  272.2 5.0 %gather_fusion.2 = bf16[768,512]{1,0:T(8,128)(2,1)} fusion(bf16[1536,512]{1,0:T(8,128)(2,1)} %bitcast.14, s32[1024]{0:T(1024)S(1)} %pad_clamp_fusion.1), kind=kCustom, calls=%fused_computation.2 | custom fusion | bytes 1575936 | tf_op jit(solution)/shard_map/gather | solution.py:197
  277.1 2.9 reshape.141
  280.1 4.2 %reduce_sum.42 = f32[384,512]{1,0:T(8,128)} reduce(f32[384,2,512]{2,1,0:T(2,128)} %reshape.141, f32[]{:T(128)} %constant.51.clone.1), dimensions={1}, to_apply=%region_7.8 | reduce | flops 196608 | bytes 2359300 | tf_op jit(solution)/shard_map/reduce_sum | solution.py:196
  295.3 8.9 %all-gather.8.cloned.1.call-done = bf16[384,2048]{1,0:T(8,128)(2,1)} async-done(((bf16[384,512]{1,0:T(8,128)(2,1)}), bf16[384,2048]{1,0:T(8,128)(2,1)}) %all-gather.8.cloned.1.call-update) | async-done | bytes 1572880 | tf_op jit(solution)/shard_map/all_gather | solution.py:261
  304.2 5.8 %convolution_convert_fusion = bf16[2048,704]{0,1:T(8,128)(2,1)} fusion(bf16[384,2048]{1,0:T(8,128)(2,1)} %all-gather.8.cloned.1.call-done, bf16[384,704]{1,0:T(8,128)(2,1)S(1)} %copy.59.pre_ref, bf16[384,704]{1,0:T(8,128)(2,1)} %copy.62.si_ref, f32[384,704]{1,0:T(8,128)} %copy.61.sb_ref, f32[384,704]{1,0:T(8,128)} %copy.60.ld_ref), kind=kOutput, calls=%fused_computation.8 | convolution fusion | flops 1112522752 | bytes 7700480 | tf_op jit(solution)/shard_map/dot_general | solution.py:267
  310.0 6.3 %convolution_bitcast_fusion.2 = f32[1,2048,256]{2,1,0:T(8,128)} fusion(bf16[1536,2048]{1,0:T(8,128)(2,1)} %bitcast.57, bf16[1536,256]{1,0:T(8,128)(2,1)} %copy-done.3), kind=kOutput, calls=%fused_computation.13 | convolution fusion | flops 1610612736 | bytes 9175040 | tf_op jit(solution)/shard_map/dot_general | solution.py:168
  316.4 6.4 %convolution_bitcast_fusion.1 = f32[1,2048,256]{2,1,0:T(8,128)} fusion(bf16[1536,2048]{1,0:T(8,128)(2,1)} %bitcast.58, bf16[1536,256]{1,0:T(8,128)(2,1)S(1)} %copy-done.8), kind=kOutput, calls=%fused_computation.12 | convolution fusion | flops 1610612736 | bytes 9175040 | tf_op jit(solution)/shard_map/dot_general | solution.py:171
  322.8 3.2 convolution_bitcast_fusion
  328.5 5.8 %local_recurrence.1 = (bf16[384,704]{1,0:T(8,128)(2,1)}, f32[384,704]{1,0:T(8,128)}, f32[384,704]{1,0:T(8,128)}, f32[8,704]{1,0:T(8,128)}) custom-call(f32[384,704]{1,0:T(8,128)} %fusion.38.dm_ref, bf16[384,704]{1,0:T(8,128)(2,1)} %copy-done.2, f32[384,704]{1,0:T(8,128)} %copy.60.ld_ref, f32[384,704]{1,0:T(8,128)} %copy.61.sb_ref, bf16[384,704]{1,0:T(8,128)(2,1)} %copy.62.si_ref), custom_call_target="tpu_custom_call" | custom-call | flops 16220160 | bytes 7569408 | tf_op jit(solution)/shard_map/local_recurrence/pallas_call | solution.py:81
  334.3 15.4 %carry_exchange.1 = f32[8,704]{1,0:T(8,128)} custom-call(f32[8,704]{1,0:T(8,128)} %get-tuple-element.14.edge_ref), custom_call_target="tpu_custom_call" | custom-call | flops 20000 | bytes 8000000 | tf_op jit(solution)/shard_map/carry_exchange/pallas_call | solution.py:135
  352.6 4.1 %multiply_multiply_fusion = (f32[384,704]{1,0:T(8,128)}, f32[384,704]{1,0:T(8,128)}) fusion(f32[384,704]{1,0:T(8,128)} %copy.61.sb_ref, f32[384,704]{1,0:T(8,128)} %copy.60.ld_ref, f32[384,704]{1,0:T(8,128)} %get-tuple-element.12, f32[384,704]{1,0:T(8,128)} %get-tuple-element.13, f32[704]{0:T(1024)S(1)} %slice_reduce_fusion), kind=kLoop, calls=%fused_computation.30 | loop fusion | flops 1081344 | bytes 6490880 | tf_op jit(solution)/shard_map/mul | solution.py:279
  361.9 24.9 %reduce-scatter.5.cloned.1.call-done = bf16[256,704]{0,1:T(8,128)(2,1)} async-done(((bf16[2048,704]{0,1:T(8,128)(2,1)}), bf16[256,704]{0,1:T(8,128)(2,1)}) %reduce-scatter.5.cloned.1.call-update) | async-done | bytes 360464 | tf_op jit(solution)/shard_map/reduce_scatter | solution.py:266
  (87 shorter events, 36.9 us)
Async XLA Ops:
  7.2 318.9 %copy-start = (bf16[2048,704]{0,1:T(8,128)(2,1)S(1)}, bf16[2048,704]{0,1:T(8,128)(2,1)}, u32[]{:S(2)}) copy-start(bf16[2048,704]{0,1:T(8,128)(2,1)} %param.19) | copy-start | bytes 8650756
  7.2 106.5 %all-gather.4.cloned.1.call-start = ((), (), s32[]{:S(2)}) async-start(), calls=%async_computation.5 | async-start | bytes 7864320 | tf_op jit(solution)/shard_map/all_gather | solution.py:243
  63.8 95.1 %all-gather.6.cloned.1.call-start = ((), (), s32[]{:S(2)}) async-start(), calls=%async_computation.6 | async-start | bytes 7864320 | tf_op jit(solution)/shard_map/all_gather | solution.py:244
  64.9 5.4 %copy-start.10 = (f32[384,2]{0,1:T(2,128)S(1)}, f32[384,2]{0,1:T(2,128)}, u32[]{:S(2)}) copy-start(f32[384,2]{0,1:T(2,128)} %param.15) | copy-start | bytes 9220
  113.4 116.3 %reduce-scatter.3.cloned.1.call-start = ((), (), s32[]{:S(2)}) async-start(), calls=%async_computation.7 | async-start | bytes 7864320 | tf_op jit(solution)/shard_map/reduce_scatter | solution.py:253
  113.7 6.2 %copy-start.5 = (bf16[1,2048,256]{2,1,0:T(8,128)(2,1)S(1)}, bf16[1,2048,256]{2,1,0:T(8,128)(2,1)}, u32[]{:S(2)}) copy-start(bf16[1,2048,256]{2,1,0:T(8,128)(2,1)} %param.17) | copy-start | bytes 3145732
  113.7 6.1 %copy-start.11 = (bf16[8,192,2048]{2,1,0:T(8,128)(2,1)S(1)}, bf16[8,192,2048]{2,1,0:T(8,128)(2,1)}, u32[]{:S(2)}) copy-start(bf16[8,192,2048]{2,1,0:T(8,128)(2,1)} %all-gather.4.cloned.1.call-done) | copy-start | bytes 18874372
  158.9 6.4 %copy-start.4 = (bf16[1,2048,256]{2,1,0:T(8,128)(2,1)S(1)}, bf16[1,2048,256]{2,1,0:T(8,128)(2,1)}, u32[]{:S(2)}) copy-start(bf16[1,2048,256]{2,1,0:T(8,128)(2,1)} %param.16) | copy-start | bytes 3145732
  165.3 1.9 copy-start.3
  165.3 1.9 copy-start.7
  165.3 1.9 copy-start.6
  171.6 63.8 %copy-start.9 = (s32[384,2]{0,1:T(2,128)S(1)}, s32[384,2]{0,1:T(2,128)}, u32[]{:S(2)}) copy-start(s32[384,2]{0,1:T(2,128)} %param.14) | copy-start | bytes 9220
  229.7 42.5 %all-to-all-start.2 = ((bf16[8,192,512]{2,1,0:T(8,128)(2,1)}), bf16[8,192,512]{2,1,0:T(8,128)(2,1)}, u32[]{:S(2)}, u32[]{:S(2)}) async-start(bf16[8,192,512]{2,1,0:T(8,128)(2,1)} %reduce-scatter.3.cloned.1.call-done), calls=%async_computation.3 | async-start | bytes 3145728 | tf_op jit(solution)/shard_map/all_to_all | solution.py:259
  235.2 69.0 %all-gather.8.cloned.1.call-start = ((), (), s32[]{:S(2)}) async-start(), calls=%async_computation.8 | async-start | bytes 1966080 | tf_op jit(solution)/shard_map/all_gather | solution.py:261
  280.1 4.2 %copy-start.1 = (bf16[384,512]{1,0:T(8,128)(2,1)S(1)}, bf16[384,512]{1,0:T(8,128)(2,1)}, u32[]{:S(2)}) copy-start(bf16[384,512]{1,0:T(8,128)(2,1)} %get-tuple-element.40) | copy-start | bytes 1179652
  286.3 100.6 %reduce-scatter.5.cloned.1.call-start = ((), (), s32[]{:S(2)}) async-start(), calls=%async_computation.9 | async-start | bytes 3244032 | tf_op jit(solution)/shard_map/reduce_scatter | solution.py:266
  287.6 16.6 %copy-start.2 = (bf16[384,704]{1,0:T(8,128)(2,1)}, bf16[384,704]{1,0:T(8,128)(2,1)S(1)}, u32[]{:S(2)}) copy-start(bf16[384,704]{1,0:T(8,128)(2,1)S(1)} %copy.59.pre_ref) | copy-start | bytes 1622020
  310.0 6.3 %copy-start.8 = (bf16[1536,256]{1,0:T(8,128)(2,1)S(1)}, bf16[1536,256]{1,0:T(8,128)(2,1)}, u32[]{:S(2)}) copy-start(bf16[1536,256]{1,0:T(8,128)(2,1)} %copy-done.7) | copy-start | bytes 2359300
  310.0 12.7 %slice-start = ((s8[6291456]{0:T(1024)(128)(4,1)}), s8[4194304]{0:T(1024)(128)(4,1)S(1)}, s32[]{:S(2)}) async-start(s8[6291456]{0:T(1024)(128)(4,1)} %bitcast.61), calls=%async_computation.10 | async-start | bytes 8388608
  316.4 6.4 %slice-start.1 = ((s8[6291456]{0:T(1024)(128)(4,1)}), s8[2097152]{0:T(1024)(128)(4,1)S(1)}, s32[]{:S(2)}) async-start(s8[6291456]{0:T(1024)(128)(4,1)} %bitcast.61), calls=%async_computation.11 | async-start | bytes 4194304
  316.4 6.4 %copy-start.13 = (f32[1536,256]{1,0:T(8,128)S(1)}, f32[1536,256]{1,0:T(8,128)}, u32[]{:S(2)}) copy-start(f32[1536,256]{1,0:T(8,128)} %fusion.12) | copy-start | bytes 4718596
  316.4 6.4 %copy-start.14 = (f32[1536,256]{1,0:T(8,128)S(1)}, f32[1536,256]{1,0:T(8,128)}, u32[]{:S(2)}) copy-start(f32[1536,256]{1,0:T(8,128)} %fusion.15) | copy-start | bytes 4718596
  322.8 3.2 copy-start.12
Sparse Core Ops, SparseCore 0:
  63.9 45.3 all-gather.3
  113.5 45.3 all-gather.5
  171.8 57.8 reduce-scatter.2
  286.4 17.7 all-gather.7
  310.1 76.6 reduce-scatter.4

commit v2 on v1

--- a/solution.py
+++ b/solution.py
@@ -151,52 +151,57 @@
     return arriving[0:1]
 
 
-def expert_work(in_rows, cot_rows, gate_w, up_w, down_w):
+def mixed_kernel(pre_ref, ld_ref, sb_ref, si_ref, out_ref):
+    pre = pre_ref[...].astype(jnp.float32)
+    half = 0.5 * (1.0 + jnp.tanh(TANH_SCALE * (pre + CUBIC * pre * pre * pre)))
+    states = jnp.exp(ld_ref[...]) * sb_ref[...] + si_ref[...].astype(jnp.float32)
+    out_ref[...] = (pre * half * states).astype(jnp.bfloat16)
+
+
+def mixed_of(gate_pre, log_decay, state_before, step_input):
+    tokens, channels = gate_pre.shape
+    steps = tokens // 32 if tokens % 32 == 0 else 1
+    block = pl.BlockSpec((tokens // steps, channels), lambda i: (i, 0))
+    return pl.pallas_call(
+        mixed_kernel,
+        grid=(steps,),
+        in_specs=[block] * 4,
+        out_specs=block,
+        out_shape=jax.ShapeDtypeStruct((tokens, channels), jnp.bfloat16),
+        compiler_params=pltpu.CompilerParams(dimension_semantics=("arbitrary",)),
+        cost_estimate=pl.CostEstimate(
+            flops=20 * tokens * channels,
+            bytes_accessed=14 * tokens * channels,
+            transcendentals=2 * tokens * channels,
+        ),
+        name="mixed",
+    )(gate_pre, log_decay, state_before, step_input)
+
+
+def transposed_dot(left, right):
+    return lax.dot_general(
+        left, right, (((0,), (0,)), ((), ())), preferred_element_type=jnp.float32
+    )
+
+
+def dot_transposed(left, right):
+    return lax.dot_general(
+        left, right, (((1,), (1,)), ((), ())), preferred_element_type=jnp.float32
+    )
+
+
+def expert_grad_of(in_rows, cot_rows, gate_w, up_w, down_w):
     gate_act = jnp.dot(in_rows, gate_w, preferred_element_type=jnp.float32)
     up_act = jnp.dot(in_rows, up_w, preferred_element_type=jnp.float32)
     sigmoid_a = jax.nn.sigmoid(gate_act)
-    hidden = (jax.nn.silu(gate_act) * up_act).astype(jnp.bfloat16)
-    grad_down = lax.dot_general(
-        hidden, cot_rows, (((0,), (0,)), ((), ())), preferred_element_type=jnp.float32
-    )
-    d_hidden = lax.dot_general(
-        cot_rows, down_w, (((1,), (1,)), ((), ())), preferred_element_type=jnp.float32
-    )
+    silu = gate_act * sigmoid_a
+    hidden = (silu * up_act).astype(jnp.bfloat16)
+    d_hidden = dot_transposed(cot_rows, down_w)
     slope = sigmoid_a * (1.0 + gate_act * (1.0 - sigmoid_a))
     d_gate_act = (d_hidden * up_act * slope).astype(jnp.bfloat16)
-    d_up_act = (d_hidden * jax.nn.silu(gate_act)).astype(jnp.bfloat16)
-    grad_gate = lax.dot_general(
-        in_rows, d_gate_act, (((0,), (0,)), ((), ())), preferred_element_type=jnp.float32
-    )
-    grad_up = lax.dot_general(
-        in_rows, d_up_act, (((0,), (0,)), ((), ())), preferred_element_type=jnp.float32
-    )
-    partial_value = lax.dot_general(
-        d_gate_act, gate_w, (((1,), (1,)), ((), ())), preferred_element_type=jnp.float32
-    )
-    partial_value = partial_value + lax.dot_general(
-        d_up_act, up_w, (((1,), (1,)), ((), ())), preferred_element_type=jnp.float32
-    )
-    rounded = lax.optimization_barrier(partial_value.astype(jnp.bfloat16))
-    return (grad_gate[None], grad_up[None], grad_down[None], rounded.astype(jnp.float32))
-
-
-def gather_slots(resid_part, cot_part, slot_token, slot_weight, groups, capacity):
-    col_width = resid_part.shape[1]
-    resid_pad = jnp.concatenate([resid_part, jnp.zeros((1, col_width), jnp.bfloat16)], axis=0)
-    cot_pad = jnp.concatenate([cot_part, jnp.zeros((1, col_width), jnp.bfloat16)], axis=0)
-    send_rows = resid_pad[slot_token].reshape(groups, capacity, col_width)
-    send_cot = (slot_weight[:, None] * cot_pad[slot_token].astype(jnp.float32)).astype(jnp.bfloat16)
-    return (send_rows, send_cot.reshape(groups, capacity, col_width))
-
-
-def combine_slots(returned, cot_part, slot_ids, tok_rows, top_count):
-    col_width = returned.shape[2]
-    flat_back = returned.reshape(-1, col_width)
-    routed = jnp.sum(
-        flat_back[slot_ids].astype(jnp.float32).reshape(tok_rows, top_count, col_width), axis=1
-    )
-    return (cot_part.astype(jnp.float32) + routed).astype(jnp.bfloat16)
+    d_up_act = (d_hidden * silu).astype(jnp.bfloat16)
+    partial_value = dot_transposed(d_gate_act, gate_w) + dot_transposed(d_up_act, up_w)
+    return partial_value.astype(jnp.bfloat16), hidden, d_gate_act, d_up_act
 
 
 def on_device(
@@ -217,60 +222,95 @@
     top_count = routes.shape[1]
     groups = lax.axis_size("sp")
     capacity = 2 * tok_rows * top_count // groups
+    pieces = 2
+    part_rows = capacity // pieces
     flat_ids = routes.reshape(-1)
     onehot = (flat_ids[:, None] == jnp.arange(groups, dtype=jnp.int32)[None, :]).astype(jnp.int32)
     ranking = jnp.sum((jnp.cumsum(onehot, axis=0) - onehot) * onehot, axis=1)
-    slot_ids = flat_ids * capacity + ranking
-    member = slot_ids[None, :] == jnp.arange(groups * capacity, dtype=jnp.int32)[:, None]
-    token_ids = jnp.arange(tok_rows * top_count, dtype=jnp.int32) // top_count
-    filled = jnp.any(member, axis=1)
-    slot_token = jnp.where(
-        filled, jnp.sum(jnp.where(member, token_ids[None, :], 0), axis=1), tok_rows
-    )
-    slot_weight = jnp.sum(jnp.where(member, route_weight.reshape(-1)[None, :], 0.0), axis=1)
+    slot_ids = (flat_ids * capacity + ranking).reshape(tok_rows, top_count)
     col_width = model_width // lax.axis_size("tp")
     col_start = lax.axis_index("tp") * col_width
     cot_part = lax.dynamic_slice_in_dim(cotangent, col_start, col_width, 1)
     resid_part = lax.dynamic_slice_in_dim(resid, col_start, col_width, 1)
-    send_rows, send_cot = gather_slots(
-        resid_part, cot_part, slot_token, slot_weight, groups, capacity
-    )
-    got_rows, got_cot = (
-        lax.all_to_all(send_rows, "sp", split_axis=0, concat_axis=0, tiled=True),
-        lax.all_to_all(send_cot, "sp", split_axis=0, concat_axis=0, tiled=True),
-    )
-    full_rows, full_cot = (
-        lax.all_gather(got_rows, "tp", axis=2, tiled=True),
-        lax.all_gather(got_cot, "tp", axis=2, tiled=True),
-    )
-    grad_gate, grad_up, grad_down, partial_value = expert_work(
-        full_rows.reshape(-1, model_width),
-        full_cot.reshape(-1, model_width),
-        w_gate[0],
-        w_up[0],
-        w_down[0],
-    )
-    summed = lax.psum_scatter(
-        partial_value.reshape(groups, capacity, model_width).astype(jnp.bfloat16),
-        "tp",
-        scatter_dimension=2,
-        tiled=True,
-    )
-    returned = lax.all_to_all(summed, "sp", split_axis=0, concat_axis=0, tiled=True)
-    part_grad = combine_slots(returned, cot_part, slot_ids, tok_rows, top_count)
+    group_base = jnp.arange(groups, dtype=jnp.int32)[:, None] * capacity
+    sends = []
+    members = []
+    for piece in range(pieces):
+        slots = group_base + piece * part_rows + jnp.arange(part_rows, dtype=jnp.int32)[None, :]
+        slots = slots.reshape(-1)
+        match = [slots[:, None] == slot_ids[None, :, k] for k in range(top_count)]
+        weight = sum(
+            jnp.sum(jnp.where(m, route_weight[None, :, k], 0.0), axis=1)
+            for k, m in enumerate(match)
+        )
+        member = functools.reduce(jnp.logical_or, match).astype(jnp.bfloat16)
+        members.append(member)
+        rows = jnp.dot(member, resid_part, preferred_element_type=jnp.float32)
+        cots = jnp.dot(member, cot_part, preferred_element_type=jnp.float32)
+        sends.append(
+            (
+                rows.astype(jnp.bfloat16).reshape(groups, part_rows, col_width),
+                (weight[:, None] * cots)
+                .astype(jnp.bfloat16)
+                .reshape(groups, part_rows, col_width),
+            )
+        )
+
+    def exchange(x):
+        return lax.all_to_all(x, "sp", split_axis=0, concat_axis=0, tiled=True)
+
+    def widen(x):
+        return lax.all_gather(x, "tp", axis=2, tiled=True)
+
+    got = []
+    token = None
+    for rows, cots in sends:
+        for x in (rows, cots):
+            if token is not None:
+                x, token = lax.optimization_barrier((x, token))
+            token = exchange(x)
+            got.append(token)
+    full = [widen(x) for x in got]
+    full[0], full[1], _ = lax.optimization_barrier((full[0], full[1], got[-1]))
+    acts = []
+    summed = []
+    for piece in range(pieces):
+        in_rows = full[2 * piece].reshape(-1, model_width)
+        cot_rows = full[2 * piece + 1].reshape(-1, model_width)
+        partial_value, hidden, d_gate_act, d_up_act = expert_grad_of(
+            in_rows, cot_rows, w_gate[0], w_up[0], w_down[0]
+        )
+        acts.append((in_rows, cot_rows, hidden, d_gate_act, d_up_act))
+        summed.append(
+            lax.psum_scatter(
+                partial_value.reshape(groups, part_rows, model_width),
+                "tp",
+                scatter_dimension=2,
+                tiled=True,
+            )
+        )
+    grad_gate = sum(transposed_dot(i, g) for i, c, h, g, u in acts)
+    grad_up = sum(transposed_dot(i, u) for i, c, h, g, u in acts)
+    grad_down = sum(transposed_dot(h, c) for i, c, h, g, u in acts)
+    mixed = mixed_of(gate_pre, log_decay, state_before, step_input)
+    summed[-1], grad_gate, grad_up, grad_down, mixed = lax.optimization_barrier(
+        (summed[-1], grad_gate, grad_up, grad_down, mixed)
+    )
+    returned = [exchange(x) for x in summed]
+    routed = sum(
+        transposed_dot(member, back.reshape(-1, col_width))
+        for member, back in zip(members, returned)
+    )
+    part_grad = (cot_part.astype(jnp.float32) + routed).astype(jnp.bfloat16)
     resid_grad = lax.all_gather(part_grad, "tp", axis=1, tiled=True)
     decays = jnp.exp(log_decay)
-    states = decays * state_before + step_input.astype(jnp.float32)
-    mixed = (jax.nn.gelu(gate_pre.astype(jnp.float32)) * states).astype(jnp.bfloat16)
-    d_mixed = jnp.dot(resid_grad, out_proj, preferred_element_type=jnp.float32)
     grad_proj = lax.psum_scatter(
-        lax.dot_general(
-            resid_grad, mixed, (((0,), (0,)), ((), ())), preferred_element_type=jnp.float32
-        ).astype(jnp.bfloat16),
+        transposed_dot(resid_grad, mixed).astype(jnp.bfloat16),
         "sp",
         scatter_dimension=0,
         tiled=True,
     ).astype(jnp.float32)
+    d_mixed = jnp.dot(resid_grad, out_proj, preferred_element_type=jnp.float32)
     grad_gate_pre, local_vals, products, edge = local_recurrence(
         d_mixed, gate_pre, log_decay, state_before, step_input
     )
@@ -278,9 +318,9 @@
     grad_step_input = local_vals + products * arriving
     grad_log_decay = grad_step_input * decays * state_before
     return (
-        grad_gate,
-        grad_up,
-        grad_down,
+        grad_gate[None],
+        grad_up[None],
+        grad_down[None],
         grad_proj,
         grad_gate_pre,
         grad_step_input,

time: 396 us -> 378 us (0.955)
  waiting for transfers between devices: 164 us -> 128 us
  local copies, waits for them, and re-layouts: 41 us -> 23.7 us
  matrix products: 46 us -> 60.8 us
  blocking collectives: 84.6 us -> 97.1 us
  Pallas kernels: 21.2 us -> 30.7 us
  other arithmetic: 17.8 us -> 9.61 us
  starting transfers between devices: 6.11 us -> 11.5 us
    all_to_all x1 -> x2, waiting for transfers between devices: 36.3 us -> 17.4 us  [exchange(): return lax.all_to_all(x, 'sp', split_axis=0, concat_axis=0, tiled=True)]
    gather x3 -> x0, local copies, waits for them, and re-layouts: 15.8 us -> none  [the longest x1 5.41 us: gather_slots(): send_rows = resid_pad[slot_token].reshape(groups, capacity, col_width)]
    reduce_scatter x2 -> x3, waiting for transfers between devices: 83 us -> 69 us  [the longest x1 39.3 us: on_device(): lax.psum_scatter(transposed_dot(resid_grad, mixed).astype(jnp.bfloat16),...]
    dot_general x9 -> x23, matrix products: 43.5 us -> 56.9 us  [the longest x9 27.6 us: transposed_dot(): lax.dot_general(left, right, (((0,), (0,)), ((), ())), preferred_element_...]
    all_to_all x2 -> x4, blocking collectives: 84.6 us -> 97.1 us  [exchange(): return lax.all_to_all(x, 'sp', split_axis=0, concat_axis=0, tiled=True)]
    all_gather x2 -> x4, waiting for transfers between devices: 36.1 us -> 24 us  [widen(): return lax.all_gather(x, 'tp', axis=2, tiled=True)]
    all_gather x1, waiting for transfers between devices: 8.93 us -> 17.7 us  [on_device(): resid_grad = lax.all_gather(part_grad, 'tp', axis=1, tiled=True)]
    pallas_call x0 -> x1, Pallas kernels: none -> 7.87 us  [mixed_of(): pl.pallas_call(mixed_kernel, grid=(steps,), in_specs=[block] * 4, out_spe...]
  transfers between devices with their start and end apart: 6 -> 10, of which waited for: 5 -> 7; matrix products, arithmetic and copies ran while one was open for 15% -> 19% of each run, Pallas kernels for 5% -> 8%
where the time goes in v2:
time: 378 us; the launch traced here: 376 us
  waiting for transfers between devices  128 us (34%)
  blocking collectives  97.1 us (26%)
  matrix products  60.8 us (16%)
  Pallas kernels  30.7 us (8%)
  local copies, waits for them, and re-layouts  23.7 us (6%)
  between operations  14.5 us (4%)
  starting transfers between devices  11.5 us (3%)
  other arithmetic  9.61 us (3%)
    all_to_all x4, blocking collectives, exchange(): return lax.all_to_all(x, 'sp', split_axis=0, concat_axis=0, tiled=True)  97.1 us
    reduce_scatter x1, waiting for transfers between devices, on_device(): lax.psum_scatter(transposed_dot(resid_grad, mixed).astype(jnp.bfloat16),...  39.3 us
    reduce_scatter x2, waiting for transfers between devices, on_device(): lax.psum_scatter(partial_value.reshape(groups, part_rows, model_width), '...  29.8 us
    dot_general x9, matrix products, transposed_dot(): lax.dot_general(left, right, (((0,), (0,)), ((), ())), preferred_element_...  27.6 us
    all_gather x4, waiting for transfers between devices, widen(): return lax.all_gather(x, 'tp', axis=2, tiled=True)  24 us
    unnamed x64, local copies, waits for them, and re-layouts  21.9 us
    all_gather x1, waiting for transfers between devices, on_device(): resid_grad = lax.all_gather(part_grad, 'tp', axis=1, tiled=True)  17.7 us
    all_to_all x2, waiting for transfers between devices, exchange(): return lax.all_to_all(x, 'sp', split_axis=0, concat_axis=0, tiled=True)  17.4 us
  transfers between devices with their start and end apart: 10, of which 7 were waited for; matrix products, arithmetic and copies ran while one was open for 19% of the time, Pallas kernels for 8%

profile of v2, /device:TPU:0, one launch (start us, length us, event | category | flops | bytes accessed | tf_op | source)
XLA Modules:
  0.0 376.2 jit_solution(14807971052153043414)
XLA Ops:
  13.6 27.3 %all_to_all.30 = bf16[8,96,512]{2,1,0:T(8,128)(2,1)} all-to-all(bf16[8,96,512]{2,1,0:T(8,128)(2,1)S(1)} %bitcast.91), channel_id=1, replica_groups=mesh['sp'=8,'tp'=4] {'sp'}, dimensions={0} | all-to-all | bytes 1572864 | tf_op jit(solution)/shard_map/all_to_all | solution.py:260
  43.5 23.3 %all_to_all.31 = bf16[8,96,512]{2,1,0:T(8,128)(2,1)} all-to-all(bf16[8,96,512]{2,1,0:T(8,128)(2,1)S(1)} %bitcast.89), channel_id=1, replica_groups=mesh['sp'=8,'tp'=4] {'sp'}, dimensions={0} | all-to-all | bytes 1572864 | tf_op jit(solution)/shard_map/all_to_all | solution.py:260
  68.5 23.2 %all_to_all.32 = bf16[8,96,512]{2,1,0:T(8,128)(2,1)} all-to-all(bf16[8,96,512]{2,1,0:T(8,128)(2,1)S(1)} %bitcast.92), channel_id=1, replica_groups=mesh['sp'=8,'tp'=4] {'sp'}, dimensions={0} | all-to-all | bytes 1572864 | tf_op jit(solution)/shard_map/all_to_all | solution.py:260
  93.4 23.2 %all_to_all.33 = bf16[8,96,512]{2,1,0:T(8,128)(2,1)} all-to-all(bf16[8,96,512]{2,1,0:T(8,128)(2,1)S(1)} %bitcast.90), channel_id=1, replica_groups=mesh['sp'=8,'tp'=4] {'sp'}, dimensions={0} | all-to-all | bytes 1572864 | tf_op jit(solution)/shard_map/all_to_all | solution.py:260
  116.8 3.3 fusion.15
  128.8 4.2 %fusion.12 = f32[768,256]{1,0:T(8,128)} fusion(bf16[768,2048]{1,0:T(8,128)(2,1)} %bitcast.78, bf16[1,2048,256]{2,1,0:T(8,128)(2,1)} %param.16), kind=kOutput, calls=%fused_computation.31 | convolution fusion | flops 805306368 | bytes 4980736 | tf_op jit(solution)/shard_map/dot_general | solution.py:194
  134.9 23.9 %all-gather.6.cloned.1.call-done = bf16[8,96,2048]{2,1,0:T(8,128)(2,1)} async-done(((bf16[8,96,512]{2,1,0:T(8,128)(2,1)}), bf16[8,96,2048]{2,1,0:T(8,128)(2,1)}) %all-gather.6.cloned.1.call-update) | async-done | bytes 3145744 | tf_op jit(solution)/shard_map/all_gather | solution.py:263
  158.8 3.9 %multiply_convert_fusion.6 = (bf16[768,256]{1,0:T(8,128)(2,1)S(1)}, bf16[768,256]{1,0:T(8,128)(2,1)S(1)}) fusion(f32[768,256]{1,0:T(8,128)} %fusion.12, f32[768,256]{1,0:T(8,128)} %fusion.18, bf16[768,2048]{1,0:T(8,128)(2,1)} %bitcast.86, bf16[1,256,2048]{2,1,0:T(8,128)(2,1)} %param.18), kind=kOutput, calls=%fused_computation.49 | convolution fusion | flops 807862272 | bytes 6553600 | tf_op jit(solution)/shard_map/dot_general | solution.py:188
  176.3 7.9 %mixed.1 = bf16[384,704]{1,0:T(8,128)(2,1)} custom-call(bf16[384,704]{1,0:T(8,128)(2,1)} %copy.100.pre_ref, f32[384,704]{1,0:T(8,128)} %copy.101.ld_ref, f32[384,704]{1,0:T(8,128)} %copy.102.sb_ref, bf16[384,704]{1,0:T(8,128)(2,1)} %copy.103.si_ref), custom_call_target="tpu_custom_call" | custom-call | flops 5406720 | bytes 3784704 | tf_op jit(solution)/shard_map/mixed/pallas_call | solution.py:165
  184.2 4.4 %fusion.62 = f32[2048,256]{1,0:T(8,128)} fusion(bf16[768,2048]{1,0:T(8,128)(2,1)} %bitcast.96, bf16[768,256]{1,0:T(8,128)(2,1)} %copy-done.18), kind=kOutput, calls=%fused_computation.100 | convolution fusion | flops 805306368 | bytes 5636096 | tf_op jit(solution)/shard_map/dot_general | solution.py:182
  191.0 7.9 %reduce-scatter.6.cloned.1.call-done = bf16[8,96,512]{2,1,0:T(8,128)(2,1)} async-done(((bf16[8,96,2048]{2,1,0:T(8,128)(2,1)}), bf16[8,96,512]{2,1,0:T(8,128)(2,1)}) %reduce-scatter.6.cloned.1.call-update) | async-done | bytes 786448 | tf_op jit(solution)/shard_map/reduce_scatter | solution.py:285
  198.9 5.5 %all-to-all-start.4 = ((bf16[8,96,512]{2,1,0:T(8,128)(2,1)}), bf16[8,96,512]{2,1,0:T(8,128)(2,1)}, u32[]{:S(2)}, u32[]{:S(2)}) async-start(bf16[8,96,512]{2,1,0:T(8,128)(2,1)} %reduce-scatter.6.cloned.1.call-done), calls=%async_computation.6 | async-start | bytes 1572864 | tf_op jit(solution)/shard_map/all_to_all | solution.py:260
  204.5 3.2 fusion.61
  217.2 21.9 %reduce-scatter.4.cloned.1.call-done = bf16[8,96,512]{2,1,0:T(8,128)(2,1)} async-done(((bf16[8,96,2048]{2,1,0:T(8,128)(2,1)}), bf16[8,96,512]{2,1,0:T(8,128)(2,1)}) %reduce-scatter.4.cloned.1.call-update) | async-done | bytes 786448 | tf_op jit(solution)/shard_map/reduce_scatter | solution.py:285
  239.1 5.5 %all-to-all-start.5 = ((bf16[8,96,512]{2,1,0:T(8,128)(2,1)}), bf16[8,96,512]{2,1,0:T(8,128)(2,1)}, u32[]{:S(2)}, u32[]{:S(2)}) async-start(bf16[8,96,512]{2,1,0:T(8,128)(2,1)} %reduce-scatter.4.cloned.1.call-done), calls=%async_computation.7 | async-start | bytes 1572864 | tf_op jit(solution)/shard_map/all_to_all | solution.py:260
  247.4 17.4 %all-to-all-done.5 = bf16[8,96,512]{2,1,0:T(8,128)(2,1)} async-done(((bf16[8,96,512]{2,1,0:T(8,128)(2,1)}), bf16[8,96,512]{2,1,0:T(8,128)(2,1)}, u32[]{:S(2)}, u32[]{:S(2)}) %all-to-all-start.5) | async-done | bytes 786464 | tf_op jit(solution)/shard_map/all_to_all | solution.py:260
  264.8 2.9 fusion.1
  267.8 17.7 %all-gather.14.cloned.1.call-done = bf16[384,2048]{1,0:T(8,128)(2,1)} async-done(((bf16[384,512]{1,0:T(8,128)(2,1)}), bf16[384,2048]{1,0:T(8,128)(2,1)}) %all-gather.14.cloned.1.call-update) | async-done | bytes 1572880 | tf_op jit(solution)/shard_map/all_gather | solution.py:305
  285.5 4.7 %convolution_convert_fusion = bf16[2048,704]{0,1:T(8,128)(2,1)} fusion(bf16[384,2048]{1,0:T(8,128)(2,1)} %all-gather.14.cloned.1.call-done, bf16[384,704]{1,0:T(8,128)(2,1)S(1)} %copy-done.17), kind=kOutput, calls=%fused_computation.2 | convolution fusion | flops 1108738048 | bytes 4997120 | tf_op jit(solution)/shard_map/dot_general | solution.py:182
  290.2 3.9 %fusion.63.dm_ref = f32[384,704]{1,0:T(8,128)} fusion(bf16[384,2048]{1,0:T(8,128)(2,1)} %all-gather.14.cloned.1.call-done, bf16[2048,704]{0,1:T(8,128)(2,1)S(1)} %copy-done), kind=kOutput, calls=%fused_computation.101 | convolution fusion | flops 1107296256 | bytes 5537792 | tf_op jit(solution)/shard_map/dot_general | solution.py:313
  294.1 5.9 %local_recurrence.1 = (bf16[384,704]{1,0:T(8,128)(2,1)}, f32[384,704]{1,0:T(8,128)}, f32[384,704]{1,0:T(8,128)}, f32[8,704]{1,0:T(8,128)}) custom-call(f32[384,704]{1,0:T(8,128)} %fusion.63.dm_ref, bf16[384,704]{1,0:T(8,128)(2,1)} %copy.100.pre_ref, f32[384,704]{1,0:T(8,128)} %copy.101.ld_ref, f32[384,704]{1,0:T(8,128)} %copy.102.sb_ref, ...), custom_call_target="tpu_custom_call" | custom-call | flops 16220160 | bytes 7569408 | tf_op jit(solution)/shard_map/local_recurrence/pallas_call | solution.py:81
  300.0 17.0 %carry_exchange.1 = f32[8,704]{1,0:T(8,128)} custom-call(f32[8,704]{1,0:T(8,128)} %get-tuple-element.34.edge_ref), custom_call_target="tpu_custom_call" | custom-call | flops 20000 | bytes 8000000 | tf_op jit(solution)/shard_map/carry_exchange/pallas_call | solution.py:135
  317.7 4.2 %multiply_multiply_fusion = (f32[384,704]{1,0:T(8,128)}, f32[384,704]{1,0:T(8,128)}) fusion(f32[384,704]{1,0:T(8,128)} %copy.102.sb_ref, f32[384,704]{1,0:T(8,128)} %copy.101.ld_ref, f32[384,704]{1,0:T(8,128)} %get-tuple-element.32, f32[384,704]{1,0:T(8,128)} %get-tuple-element.33, f32[704]{0:T(1024)S(1)} %slice_reduce_fusion), kind=kLoop, calls=%fused_computation.23 | loop fusion | flops 1081344 | bytes 6490880 | tf_op jit(solution)/shard_map/mul | solution.py:319
  328.2 39.3 %reduce-scatter.8.cloned.1.call-done = bf16[256,704]{0,1:T(8,128)(2,1)} async-done(((bf16[2048,704]{0,1:T(8,128)(2,1)}), bf16[256,704]{0,1:T(8,128)(2,1)}) %reduce-scatter.8.cloned.1.call-update) | async-done | bytes 360464 | tf_op jit(solution)/shard_map/reduce_scatter | solution.py:307
  (125 shorter events, 60.2 us)
Async XLA Ops:
  7.2 283.1 %copy-start = (bf16[2048,704]{0,1:T(8,128)(2,1)S(1)}, bf16[2048,704]{0,1:T(8,128)(2,1)}, u32[]{:S(2)}) copy-start(bf16[2048,704]{0,1:T(8,128)(2,1)} %param.19) | copy-start | bytes 8650756
  7.2 109.6 %all-gather.10.cloned.1.call-start = ((), (), s32[]{:S(2)}) async-start(), calls=%async_computation.12 | async-start | bytes 3932160 | tf_op jit(solution)/shard_map/all_gather | solution.py:263
  11.9 29.2 %copy-start.19 = (f32[384,2]{0,1:T(2,128)S(1)}, f32[384,2]{0,1:T(2,128)}, u32[]{:S(2)}) copy-start(f32[384,2]{0,1:T(2,128)} %param.15) | copy-start | bytes 9220
  40.9 75.9 %all-gather.12.cloned.1.call-start = ((), (), s32[]{:S(2)}) async-start(), calls=%async_computation.13 | async-start | bytes 3932160 | tf_op jit(solution)/shard_map/all_gather | solution.py:263
  66.8 62.0 %all-gather.8.cloned.1.call-start = ((), (), s32[]{:S(2)}) async-start(), calls=%async_computation.10 | async-start | bytes 3932160 | tf_op jit(solution)/shard_map/all_gather | solution.py:263
  91.7 67.0 %all-gather.6.cloned.1.call-start = ((), (), s32[]{:S(2)}) async-start(), calls=%async_computation.9 | async-start | bytes 3932160 | tf_op jit(solution)/shard_map/all_gather | solution.py:263
  116.7 82.2 %reduce-scatter.6.cloned.1.call-start = ((), (), s32[]{:S(2)}) async-start(), calls=%async_computation.14 | async-start | bytes 3932160 | tf_op jit(solution)/shard_map/reduce_scatter | solution.py:285
  128.5 110.6 %reduce-scatter.4.cloned.1.call-start = ((), (), s32[]{:S(2)}) async-start(), calls=%async_computation.11 | async-start | bytes 3932160 | tf_op jit(solution)/shard_map/reduce_scatter | solution.py:285
  128.8 4.2 %copy-start.1 = (bf16[8,96,2048]{2,1,0:T(8,128)(2,1)S(1)}, bf16[8,96,2048]{2,1,0:T(8,128)(2,1)}, u32[]{:S(2)}) copy-start(bf16[8,96,2048]{2,1,0:T(8,128)(2,1)} %all-gather.8.cloned.1.call-done) | copy-start | bytes 9437188
  128.8 4.2 %copy-start.6 = (bf16[1,2048,256]{2,1,0:T(8,128)(2,1)S(1)}, bf16[1,2048,256]{2,1,0:T(8,128)(2,1)}, u32[]{:S(2)}) copy-start(bf16[1,2048,256]{2,1,0:T(8,128)(2,1)} %param.17) | copy-start | bytes 3145732
  158.8 3.9 %copy-start.4 = (bf16[1,2048,256]{2,1,0:T(8,128)(2,1)S(1)}, bf16[1,2048,256]{2,1,0:T(8,128)(2,1)}, u32[]{:S(2)}) copy-start(bf16[1,2048,256]{2,1,0:T(8,128)(2,1)} %param.16) | copy-start | bytes 3145732
  184.2 4.4 %copy-start.22 = (bf16[8,96,2048]{2,1,0:T(8,128)(2,1)S(1)}, bf16[8,96,2048]{2,1,0:T(8,128)(2,1)}, u32[]{:S(2)}) copy-start(bf16[8,96,2048]{2,1,0:T(8,128)(2,1)} %all-gather.12.cloned.1.call-done) | copy-start | bytes 9437188
  184.2 4.4 %copy-start.25 = (f32[768,256]{1,0:T(8,128)S(1)}, f32[768,256]{1,0:T(8,128)}, u32[]{:S(2)}) copy-start(f32[768,256]{1,0:T(8,128)} %copy-done.24) | copy-start | bytes 2359300
  184.2 4.4 %copy-start.27 = (f32[768,256]{1,0:T(8,128)S(1)}, f32[768,256]{1,0:T(8,128)}, u32[]{:S(2)}) copy-start(f32[768,256]{1,0:T(8,128)} %copy-done.26) | copy-start | bytes 2359300
  198.9 40.1 %all-to-all-start.4 = ((bf16[8,96,512]{2,1,0:T(8,128)(2,1)}), bf16[8,96,512]{2,1,0:T(8,128)(2,1)}, u32[]{:S(2)}, u32[]{:S(2)}) async-start(bf16[8,96,512]{2,1,0:T(8,128)(2,1)} %reduce-scatter.6.cloned.1.call-done), calls=%async_computation.6 | async-start | bytes 1572864 | tf_op jit(solution)/shard_map/all_to_all | solution.py:260
  204.4 4.1 %copy-start.8 = (f32[2048,256]{1,0:T(8,128)S(1)}, f32[2048,256]{1,0:T(8,128)}, u32[]{:S(2)}) copy-start(f32[2048,256]{1,0:T(8,128)} %fusion.62) | copy-start | bytes 6291460
  204.5 4.2 %copy-start.12 = (bf16[768,256]{1,0:T(8,128)(2,1)S(1)}, bf16[768,256]{1,0:T(8,128)(2,1)}, u32[]{:S(2)}) copy-start(bf16[768,256]{1,0:T(8,128)(2,1)} %copy-done.11) | copy-start | bytes 1179652
  211.0 3.5 copy-start.14
  211.0 3.7 copy-start.15
  239.1 25.7 %all-to-all-start.5 = ((bf16[8,96,512]{2,1,0:T(8,128)(2,1)}), bf16[8,96,512]{2,1,0:T(8,128)(2,1)}, u32[]{:S(2)}, u32[]{:S(2)}) async-start(bf16[8,96,512]{2,1,0:T(8,128)(2,1)} %reduce-scatter.4.cloned.1.call-done), calls=%async_computation.7 | async-start | bytes 1572864 | tf_op jit(solution)/shard_map/all_to_all | solution.py:260
  244.6 40.9 %all-gather.14.cloned.1.call-start = ((), (), s32[]{:S(2)}) async-start(), calls=%async_computation.15 | async-start | bytes 1966080 | tf_op jit(solution)/shard_map/all_gather | solution.py:305
  247.4 38.1 %copy-start.17 = (bf16[384,704]{1,0:T(8,128)(2,1)S(1)}, bf16[384,704]{1,0:T(8,128)(2,1)}, u32[]{:S(2)}) copy-start(bf16[384,704]{1,0:T(8,128)(2,1)} %mixed.1) | copy-start | bytes 1622020
  267.7 99.7 %reduce-scatter.8.cloned.1.call-start = ((), (), s32[]{:S(2)}) async-start(), calls=%async_computation.16 | async-start | bytes 3244032 | tf_op jit(solution)/shard_map/reduce_scatter | solution.py:307
  321.9 5.3 %copy-start.16 = (bf16[384,704]{1,0:T(8,128)(2,1)S(1)}, bf16[384,704]{1,0:T(8,128)(2,1)}, u32[]{:S(2)}) copy-start(bf16[384,704]{1,0:T(8,128)(2,1)} %get-tuple-element.67) | copy-start | bytes 1622020
  (14 other events, 31.4 us)
Sparse Core Ops, SparseCore 0:
  41.0 27.5 all-gather.9
  70.2 28.4 all-gather.11
  100.3 28.4 all-gather.7
  130.3 28.4 all-gather.5
  161.2 37.7 reduce-scatter.5
  201.3 37.7 reduce-scatter.3
  267.9 17.6 all-gather.13
  290.3 77.0 reduce-scatter.7
